TPU v7x, 32 devices: a whole 2x2x4 slice. The times are simulated.
32 devices in a mesh: grp: 2 (over x), tp: 16 (over z, y, core).
Axes of the slice: x: 2, y: 2, z: 4, core: 2. Of those that a mesh axis runs over, the one named last changes fastest.
Arguments:
- tokens: bfloat16 [128, 4096], P('grp', 'tp'), parts along dimension 0, may hold values from -6 to 6
- lengths: int32 [128], P('grp'), parts along dimension 0, may hold values from 1 to 2048, as said below
- norm_gain: float32 [2, 4096], replicated, may hold values from 0.1 to 1.9
- in_weight: bfloat16 [2, 1024, 4096], P(None, 'tp'), may hold values from -0.09375 to 0.09375
- gate_weight: bfloat16 [2, 4096, 4096], P(None, 'tp'), may hold values from -0.09375 to 0.09375
- decay_rate: float32 [2, 64, 64], P(None, 'tp'), may hold values from 0.05 to 2
- frequency: float32 [2, 64, 64], P(None, 'tp'), may hold values from 0 to 201.06177
- log_step: float32 [2, 64], P(None, 'tp'), may hold values from -3 to 0
- input_map: float32 [2, 2, 64, 64, 16], P(None, None, 'tp'), may hold values from -1 to 1
- output_map: float32 [2, 2, 64, 16, 64], P(None, None, 'tp'), may hold values from -0.75 to 0.75
- skip_scale: float32 [2, 1024], P(None, 'tp'), may hold values from -4 to 4
- glu_weight: bfloat16 [2, 1024, 1024], P(None, 'tp'), may hold values from -0.1875 to 0.1875
- branch_weight: bfloat16 [2, 4096, 1024], P(None, 'tp'), may hold values from -0.1875 to 0.1875
- mix_weight: bfloat16 [2, 4096, 4096], P(None, 'tp'), may hold values from -0.09375 to 0.09375
- states: float32 [2, 2, 64, 64, 128], P(None, None, 'tp', None, 'grp'), parts along dimension 4, may hold values from -3 to 3
Outputs:
- mixed: bfloat16 [128, 4096], P('grp', 'tp'), parts along dimension 0
- new_states: float32 [2, 2, 64, 64, 128], P(None, None, 'tp', None, 'grp'), parts along dimension 4
There are 2 independent parts, one for each index of `grp`. A program takes and returns all parts, laid end to end along the dimension named above; an argument that names none is the same for every part. Nothing has to cross between parts.
Inputs may be any that keep to these rules, and one draw needn't show every extreme that they name: `lengths`: one length is exactly 2048. Any number of sequences, from 1 to 64, may be longer than 512.
All inputs are finite; a program needn't handle non-finite values.
Results may differ from a plain program's by a relative error of at most 0.0085.
Values may be sent and summed in bfloat16 or wider, within the bound.
A program may use at most 64 MiB of HBM per device.

v0:
```python
import jax
import jax.numpy as jnp
from jax import lax
from jax.sharding import PartitionSpec as P

LAYERS = 2
MEAN_LEN = 512


EPS = 1e-06
HIGH = lax.Precision.HIGHEST


def discretize(decay_rate, frequency, log_step, input_map):
    step_len = jnp.exp(log_step)[:, None]
    real_part = -decay_rate
    magnitude = jnp.exp(real_part * step_len)
    decay_re = magnitude * jnp.cos(frequency * step_len)
    decay_im = magnitude * jnp.sin(frequency * step_len)
    denom = real_part * real_part + frequency * frequency
    factor_re = ((decay_re - 1.0) * real_part + decay_im * frequency) / denom
    factor_im = (decay_im * real_part - (decay_re - 1.0) * frequency) / denom
    drive_re = factor_re[..., None] * input_map[0] - factor_im[..., None] * input_map[1]
    drive_im = factor_re[..., None] * input_map[1] + factor_im[..., None] * input_map[0]
    return (decay_re, decay_im, drive_re, drive_im)


def recur(drive, live, decay_rate, frequency, log_step, input_map, output_map, skip_scale, carried):
    groups = decay_rate.shape[0]
    batch = drive.shape[0]
    decay_re, decay_im, drive_re, drive_im = discretize(decay_rate, frequency, log_step, input_map)
    grouped = drive.reshape(batch, groups, -1)
    push_re = jnp.einsum("gnp,bgp->gnb", drive_re, grouped, precision=HIGH)
    push_im = jnp.einsum("gnp,bgp->gnb", drive_im, grouped, precision=HIGH)
    new_re = decay_re[..., None] * carried[0] - decay_im[..., None] * carried[1] + push_re
    new_im = decay_re[..., None] * carried[1] + decay_im[..., None] * carried[0] + push_im
    new_re = jnp.where(live[None, None, :] > 0, new_re, carried[0])
    new_im = jnp.where(live[None, None, :] > 0, new_im, carried[1])
    read = (
        jnp.einsum("gpn,gnb->bgp", output_map[0], new_re, precision=HIGH)
        - jnp.einsum("gpn,gnb->bgp", output_map[1], new_im, precision=HIGH)
        + skip_scale.reshape(groups, -1) * grouped
    )
    activated = jax.nn.gelu(read.reshape(batch, -1)).astype(jnp.bfloat16)
    return (activated, jnp.stack([new_re, new_im]))


def contract_piece(piece, weight):
    return lax.dot_general(
        piece, weight, (((1,), (1,)), ((), ())), preferred_element_type=jnp.float32
    )


def product_fold(weight, piece):
    return contract_piece(piece, weight)


def one_layer(
    current,
    live,
    norm_gain,
    in_weight,
    gate_weight,
    decay_rate,
    frequency,
    log_step,
    input_map,
    output_map,
    skip_scale,
    glu_weight,
    branch_weight,
    mix_weight,
    carried,
):
    width = current.shape[1]
    features = width * lax.axis_size("tp")
    wide_in = current.astype(jnp.float32)
    piece_wide = lax.all_gather(current, "tp", axis=1, tiled=True).astype(jnp.float32)
    scaled_piece = (piece_wide * norm_gain).astype(jnp.bfloat16)
    drive_acc = contract_piece(scaled_piece, in_weight)
    gate_acc = contract_piece(scaled_piece, gate_weight)
    drive_acc, gate_acc = (drive_acc, gate_acc)
    squares_sum = jnp.sum(piece_wide * piece_wide, axis=1)
    inv_rms = lax.rsqrt(squares_sum / features + EPS)[:, None]
    drive = inv_rms * drive_acc
    opening = jax.nn.sigmoid(inv_rms * gate_acc)
    activated, fresh = recur(
        drive, live, decay_rate, frequency, log_step, input_map, output_map, skip_scale, carried
    )
    glu_pre = product_fold(glu_weight, lax.all_gather(activated, "tp", axis=1, tiled=True))
    gated_units = (activated.astype(jnp.float32) * jax.nn.sigmoid(glu_pre)).astype(jnp.bfloat16)
    branch = product_fold(branch_weight, lax.all_gather(gated_units, "tp", axis=1, tiled=True))
    weighted = (opening * branch).astype(jnp.bfloat16)
    update = product_fold(mix_weight, lax.all_gather(weighted, "tp", axis=1, tiled=True))
    result = jnp.where(live[:, None] > 0, wide_in + update, wide_in).astype(jnp.bfloat16)
    return (result, fresh)


def run_layers(
    current,
    live,
    carried_all,
    norm_gain,
    in_weight,
    gate_weight,
    decay_rate,
    frequency,
    log_step,
    input_map,
    output_map,
    skip_scale,
    glu_weight,
    branch_weight,
    mix_weight,
):
    finals = []
    for layer in range(LAYERS):
        current, fresh = one_layer(
            current,
            live,
            norm_gain[layer],
            in_weight[layer],
            gate_weight[layer],
            decay_rate[layer],
            frequency[layer],
            log_step[layer],
            input_map[layer],
            output_map[layer],
            skip_scale[layer],
            glu_weight[layer],
            branch_weight[layer],
            mix_weight[layer],
            carried_all[layer],
        )
        finals.append(fresh)
    return (current, jnp.stack(finals))


def per_device(
    tokens,
    lengths,
    norm_gain,
    in_weight,
    gate_weight,
    decay_rate,
    frequency,
    log_step,
    input_map,
    output_map,
    skip_scale,
    glu_weight,
    branch_weight,
    mix_weight,
    states,
):
    live_all = (lengths > MEAN_LEN).astype(jnp.int32)
    weights = (
        norm_gain,
        in_weight,
        gate_weight,
        decay_rate,
        frequency,
        log_step,
        input_map,
        output_map,
        skip_scale,
        glu_weight,
        branch_weight,
        mix_weight,
    )
    mixed, new_states = run_layers(tokens, live_all, states, *weights)
    return (mixed, new_states)


def solution(mesh):
    in_specs = (
        P("grp", "tp"),
        P("grp"),
        P(),
        P(None, "tp", None),
        P(None, "tp", None),
        P(None, "tp", None),
        P(None, "tp", None),
        P(None, "tp"),
        P(None, None, "tp", None, None),
        P(None, None, "tp", None, None),
        P(None, "tp"),
        P(None, "tp", None),
        P(None, "tp", None),
        P(None, "tp", None),
        P(None, None, "tp", None, "grp"),
    )
    out_specs = (P("grp", "tp"), P(None, None, "tp", None, "grp"))
    return jax.shard_map(
        per_device, mesh=mesh, in_specs=in_specs, out_specs=out_specs, check_vma=False
    )
```

profile of v0, /device:TPU:0, one launch (start us, length us, event | category | flops | bytes accessed | tf_op | source)
XLA Modules:
  0.0 176.9 jit_solution(8379955971969608418)
XLA Ops:
  0.6 0.0 copy-start.1
  0.6 0.0 copy-start.2
  0.7 0.0 copy-start.3
  0.7 0.0 copy-start
  0.7 0.0 copy-start.9
  0.7 0.8 fusion.164
  1.5 0.8 exponential_bitcast_fusion
  2.2 0.8 slice_reduce_fusion
  3.0 0.1 mul.541
  3.1 0.1 mul.500
  3.2 0.8 fusion.155
  4.0 0.8 fusion.160
  4.9 0.7 fusion.162
  5.6 0.9 fusion.165
  6.4 24.8 %all_gather.24 = bf16[64,4096]{1,0:T(8,128)(2,1)S(1)} all-gather(bf16[64,256]{1,0:T(8,128)(2,1)} %param.15), channel_id=1, replica_groups=mesh['grp'=2,'tp'=16] {'tp'}, dimensions={1}, use_global_device_ids=true | all-gather | bytes 557056 | tf_op jit(solution)/shard_map/all_gather | solution.py:78
  31.3 0.2 fusion.80
  31.5 1.4 convolution_multiply_fusion.3
  32.8 2.4 %fusion.28 = f32[64,256]{1,0:T(8,128)S(1)} fusion(bf16[2,256,4096]{2,1,0:T(8,128)(2,1)} %param.19, bf16[64,4096]{1,0:T(8,128)(2,1)S(1)} %all_gather.24, f32[4096]{0:T(1024)S(1)} %bitcast.299, f32[64]{0:T(128)S(1)} %add_rsqrt_fusion.1), kind=kOutput, calls=%fused_computation.30 | convolution fusion | flops 135069696 | bytes 2703616 | tf_op jit(solution)/shard_map/dot_general | solution.py:49
  35.2 0.1 copy.23
  35.3 0.0 copy-start.8
  35.3 0.0 copy-done.1
  35.3 0.4 fusion.14
  35.8 0.4 fusion.15
  36.2 0.2 fusion.128
  36.4 0.2 fusion.69
  36.7 0.0 copy-start.5
  36.7 18.3 %all_gather.25 = bf16[64,1024]{0,1:T(8,128)(2,1)S(1)} all-gather(bf16[64,64]{0,1:T(8,128)(2,1)S(1)} %fusion.111), channel_id=1, replica_groups=mesh['grp'=2,'tp'=16] {'tp'}, dimensions={1}, use_global_device_ids=true | all-gather | bytes 139264 | tf_op jit(solution)/shard_map/all_gather | solution.py:90
  55.0 0.2 fusion.78
  55.2 19.5 %all_gather.26 = bf16[64,1024]{0,1:T(8,128)(2,1)S(1)} all-gather(bf16[64,64]{0,1:T(8,128)(2,1)S(1)} %fusion.78), channel_id=1, replica_groups=mesh['grp'=2,'tp'=16] {'tp'}, dimensions={1}, use_global_device_ids=true | all-gather | bytes 139264 | tf_op jit(solution)/shard_map/all_gather | solution.py:92
  74.7 0.3 fusion.64
  75.0 18.9 %all_gather.27 = bf16[64,4096]{1,0:T(8,128)(2,1)S(1)} all-gather(bf16[64,256]{1,0:T(8,128)(2,1)S(1)} %fusion.64), channel_id=1, replica_groups=mesh['grp'=2,'tp'=16] {'tp'}, dimensions={1}, use_global_device_ids=true | all-gather | bytes 557056 | tf_op jit(solution)/shard_map/all_gather | solution.py:94
  93.9 0.8 fusion.61
  94.7 20.3 %all_gather.28 = bf16[64,4096]{1,0:T(8,128)(2,1)S(1)} all-gather(bf16[64,256]{1,0:T(8,128)(2,1)S(1)} %fusion.61), channel_id=1, replica_groups=mesh['grp'=2,'tp'=16] {'tp'}, dimensions={1}, use_global_device_ids=true | all-gather | bytes 557056 | tf_op jit(solution)/shard_map/all_gather | solution.py:78
  114.9 0.2 fusion.82
  115.2 0.3 convolution_multiply_fusion.2
  115.5 0.8 fusion.49
  116.3 0.1 copy.24
  116.4 0.4 fusion.12
  116.8 0.4 fusion.13
  117.2 0.2 fusion.121
  117.4 0.2 fusion.67
  117.7 18.2 %all_gather.29 = bf16[64,1024]{0,1:T(8,128)(2,1)S(1)} all-gather(bf16[64,64]{0,1:T(8,128)(2,1)S(1)} %fusion.119), channel_id=1, replica_groups=mesh['grp'=2,'tp'=16] {'tp'}, dimensions={1}, use_global_device_ids=true | all-gather | bytes 139264 | tf_op jit(solution)/shard_map/all_gather | solution.py:90
  135.9 0.2 fusion.79
  136.0 19.5 %all_gather.30 = bf16[64,1024]{0,1:T(8,128)(2,1)S(1)} all-gather(bf16[64,64]{0,1:T(8,128)(2,1)S(1)} %fusion.79), channel_id=1, replica_groups=mesh['grp'=2,'tp'=16] {'tp'}, dimensions={1}, use_global_device_ids=true | all-gather | bytes 139264 | tf_op jit(solution)/shard_map/all_gather | solution.py:92
  155.5 0.3 fusion.65
  155.8 0.8 pad_maximum_fusion
  156.7 18.9 %all_gather.31 = bf16[64,4096]{1,0:T(8,128)(2,1)S(1)} all-gather(bf16[64,256]{1,0:T(8,128)(2,1)S(1)} %fusion.65), channel_id=1, replica_groups=mesh['grp'=2,'tp'=16] {'tp'}, dimensions={1}, use_global_device_ids=true | all-gather | bytes 557056 | tf_op jit(solution)/shard_map/all_gather | solution.py:94
  175.5 1.4 fusion.58
  (18 shorter events, 0.1 us)
Async XLA Ops:
  0.6 34.7 %copy-start.1 = (f32[2,2,4,64,64]{4,3,2,1,0:T(8,128)S(1)}, f32[2,2,4,64,64]{4,3,2,1,0:T(8,128)}, u32[]{:S(2)}) copy-start(f32[2,2,4,64,64]{4,3,2,1,0:T(8,128)} %param.29) | copy-start | bytes 786436
  0.6 35.5 %copy-start.2 = (f32[2,2,4,16,64]{4,3,2,1,0:T(8,128)S(1)}, f32[2,2,4,16,64]{4,3,2,1,0:T(8,128)}, u32[]{:S(2)}) copy-start(f32[2,2,4,16,64]{4,3,2,1,0:T(8,128)} %param.24) | copy-start | bytes 196612
  0.7 34.7 %copy-start.3 = (f32[2,2,4,64,16]{3,4,2,1,0:T(8,128)S(1)}, f32[2,2,4,64,16]{3,4,2,1,0:T(8,128)}, u32[]{:S(2)}) copy-start(f32[2,2,4,64,16]{3,4,2,1,0:T(8,128)} %param.23) | copy-start | bytes 196612
  0.7 74.0 %copy-start = (bf16[2,256,1024]{2,1,0:T(8,128)(2,1)S(1)}, bf16[2,256,1024]{2,1,0:T(8,128)(2,1)}, u32[]{:S(2)}) copy-start(bf16[2,256,1024]{2,1,0:T(8,128)(2,1)} %param.27) | copy-start | bytes 3145732
  0.7 54.3 %copy-start.9 = (bf16[2,64,1024]{2,1,0:T(8,128)(2,1)S(1)}, bf16[2,64,1024]{2,1,0:T(8,128)(2,1)}, u32[]{:S(2)}) copy-start(bf16[2,64,1024]{2,1,0:T(8,128)(2,1)} %param.26) | copy-start | bytes 786436
  31.5 62.4 %copy-start.4 = (bf16[64,256]{1,0:T(8,128)(2,1)S(1)}, bf16[64,256]{1,0:T(8,128)(2,1)}, u32[]{:S(2)}) copy-start(bf16[64,256]{1,0:T(8,128)(2,1)} %param.15) | copy-start | bytes 98308
  35.3 58.6 %copy-start.6 = (bf16[2,256,4096]{2,1,0:T(8,128)(2,1)S(1)}, bf16[2,256,4096]{2,1,0:T(8,128)(2,1)}, u32[]{:S(2)}) copy-start(bf16[2,256,4096]{2,1,0:T(8,128)(2,1)} %param.28) | copy-start | bytes 12582916
  35.3 79.9 %copy-start.8 = (bf16[2,64,4096]{2,1,0:T(8,128)(2,1)S(1)}, bf16[2,64,4096]{2,1,0:T(8,128)(2,1)}, u32[]{:S(2)}) copy-start(bf16[2,64,4096]{2,1,0:T(8,128)(2,1)} %param.18) | copy-start | bytes 3145732
  36.7 78.8 %copy-start.5 = (bf16[2,256,4096]{2,1,0:T(8,128)(2,1)S(1)}, bf16[2,256,4096]{2,1,0:T(8,128)(2,1)}, u32[]{:S(2)}) copy-start(bf16[2,256,4096]{2,1,0:T(8,128)(2,1)} %param.19) | copy-start | bytes 12582916
  116.3 59.2 %copy-start.7 = (bf16[2,256,4096]{2,1,0:T(8,128)(2,1)S(1)}, bf16[2,256,4096]{2,1,0:T(8,128)(2,1)}, u32[]{:S(2)}) copy-start(bf16[2,256,4096]{2,1,0:T(8,128)(2,1)} %param.28) | copy-start | bytes 12582916
where the time goes:
time: 177 us
  blocking collectives  158 us (89%)
  matrix products  10.5 us (6%)
  other arithmetic  4.53 us (3%)
  local copies, waits for them, and re-layouts  2.76 us (2%)
    all_gather x2, blocking collectives, one_layer(): lax.all_gather(current, 'tp', axis=1, tiled=True).astype(jnp.float32)  45.1 us
    all_gather x2, blocking collectives, one_layer(): lax.all_gather(gated_units, 'tp', axis=1, tiled=True)  39 us
    all_gather x2, blocking collectives, one_layer(): lax.all_gather(weighted, 'tp', axis=1, tiled=True)  37.7 us
    all_gather x2, blocking collectives, one_layer(): lax.all_gather(activated, 'tp', axis=1, tiled=True)  36.4 us
    dot_general x10, matrix products, contract_piece(): lax.dot_general(piece, weight, (((1,), (1,)), ((), ())), preferred_elemen...  7.91 us

commit v1 on v0

v1 whole, which is shorter than its diff:
```python
import functools

import jax
import jax.numpy as jnp
from jax import lax
from jax.experimental import pallas as pl
from jax.experimental.pallas import tpu as pltpu
from jax.sharding import PartitionSpec as P

MEAN_LEN = 512
EPS = 1e-06
HIGH = lax.Precision.HIGHEST
MESH = pl.DeviceIdType.MESH


def dot_nt(a, b, precision=None):
    return lax.dot_general(
        a, b, (((1,), (1,)), ((), ())), precision=precision, preferred_element_type=jnp.float32
    )


def dot_nn(a, b, precision=None):
    return lax.dot_general(
        a, b, (((1,), (0,)), ((), ())), precision=precision, preferred_element_type=jnp.float32
    )


def eye(n):
    return lax.broadcasted_iota(jnp.int32, (n, n), 0) == lax.broadcasted_iota(jnp.int32, (n, n), 1)


def to_col(row):
    n = row.shape[1]
    return jnp.sum(jnp.where(eye(n), jnp.broadcast_to(row, (n, n)), 0.0), axis=1, keepdims=True)


def to_row(col):
    n = col.shape[0]
    return jnp.sum(jnp.where(eye(n), jnp.broadcast_to(col, (n, n)), 0.0), axis=0, keepdims=True)


def kernel(
    dims,
    tokens,
    lengths,
    gain,
    skip,
    decay_rate,
    frequency,
    log_step,
    in_hbm,
    gate_hbm,
    input_hbm,
    output_hbm,
    glu_hbm,
    branch_hbm,
    mix_hbm,
    states_hbm,
    mixed,
    states_out,
    in_w,
    gate_w,
    glu_w,
    branch_w,
    mix_w,
    imap,
    omap,
    carried,
    xbuf,
    abuf,
    gbuf,
    wbuf,
    scaled,
    push_map,
    direct,
    base,
    load_sem,
    out_sem,
    send_sem,
    recv_sem,
):
    layers, zs, ys, cs = dims
    n = zs * ys * cs
    batch, width = tokens.shape
    features = width * n
    groups = decay_rate.shape[1]
    per = imap.shape[-1]
    chans = groups * per
    aligned = width % 128 == 0

    me = lax.axis_index("tp")
    core = lax.rem(me, cs)
    yy = lax.rem(me // cs, ys)
    zz = me // (cs * ys)

    def place(z, y, c):
        return (z * ys + y) * cs + c

    hops = sorted(range(1, zs), key=lambda d: (min(d, zs - d), d))
    across = [lax.rem(zz + d, zs) for d in hops]
    peers = [place(z, yy, core) for z in across]
    other_y = place(zz, 1 - yy, core) if ys > 1 else None
    partner = place(zz, yy, 1 - core) if cs > 1 else None
    greeted = peers + [p for p in (other_y, partner) if p is not None]

    barrier = pltpu.get_barrier_semaphore()
    for p in greeted:
        pl.semaphore_signal(barrier, inc=1, device_id={"tp": p}, device_id_type=MESH)

    def load(at, src, dst):
        copy = pltpu.make_async_copy(src, dst, load_sem.at[at])
        copy.start()
        return copy

    loads = {}
    count = 0
    plan = [("maps", None)]
    loads["imap"] = load(0, input_hbm, imap)
    loads["omap"] = load(1, output_hbm, omap)
    loads["states"] = load(2, states_hbm, carried)
    count = 3
    for layer in range(layers):
        for name, src, dst in (
            ("in", in_hbm, in_w),
            ("gate", gate_hbm, gate_w),
            ("glu", glu_hbm, glu_w),
            ("branch", branch_hbm, branch_w),
            ("mix", mix_hbm, mix_w),
        ):
            loads[name, layer] = load(count, src.at[layer], dst.at[layer])
            count += 1

    live_row = lengths[...] > MEAN_LEN
    live_row_f = jnp.where(live_row, 1.0, 0.0)
    live_col_f = to_col(live_row_f)
    live_col = live_col_f > 0.5

    sends = []

    def send(phase, buf, slot, target, slot_count):
        copy = pltpu.make_async_remote_copy(
            src_ref=buf.at[slot],
            dst_ref=buf.at[slot],
            send_sem=send_sem.at[phase, slot_count],
            recv_sem=recv_sem.at[phase, slot],
            device_id={"tp": target},
            device_id_type=MESH,
        )
        copy.start()
        sends.append(copy)

    def start(phase, buf):
        k = 0
        for p in list(reversed(peers)) + [p for p in (other_y, partner) if p is not None]:
            send(phase, buf, me, p, k)
            k += 1
        return k

    def arrive(phase, buf, slot):
        pltpu.make_async_remote_copy(
            src_ref=buf.at[slot],
            dst_ref=buf.at[slot],
            send_sem=send_sem.at[phase, 0],
            recv_sem=recv_sem.at[phase, slot],
            device_id={"tp": greeted[0]},
            device_id_type=MESH,
        ).wait_recv()

    def finish(phase, buf, k, each=None):
        def take(slot):
            if each is not None:
                each(slot)

        if each is not None:
            each(me)
        if ys > 1:
            arrive(phase, buf, other_y)
            if cs > 1:
                send(phase, buf, other_y, partner, k)
                k += 1
            take(other_y)
        for z in across:
            slot = place(z, yy, core)
            arrive(phase, buf, slot)
            if ys > 1:
                send(phase, buf, slot, other_y, k)
                k += 1
            if cs > 1:
                send(phase, buf, slot, partner, k)
                k += 1
            take(slot)
        if ys > 1:
            for z in across:
                slot = place(z, 1 - yy, core)
                arrive(phase, buf, slot)
                if cs > 1:
                    send(phase, buf, slot, partner, k)
                    k += 1
                take(slot)
        if cs > 1:
            order = [place(zz, yy, 1 - core)]
            if ys > 1:
                order.append(place(zz, 1 - yy, 1 - core))
            order += [place(z, yy, 1 - core) for z in across]
            if ys > 1:
                order += [place(z, 1 - yy, 1 - core) for z in across]
            for slot in order:
                arrive(phase, buf, slot)
                take(slot)

    def prepare(layer):
        step = log_step[layer : layer + 1, :]
        step_len = jnp.exp(to_col(step) if groups > 1 else step)
        real = -decay_rate[layer]
        freq = frequency[layer]
        magnitude = jnp.exp(real * step_len)
        decay_re = magnitude * jnp.cos(freq * step_len)
        decay_im = magnitude * jnp.sin(freq * step_len)
        denom = real * real + freq * freq
        factor_re = ((decay_re - 1.0) * real + decay_im * freq) / denom
        factor_im = (decay_im * real - (decay_re - 1.0) * freq) / denom
        res, ims, bases = [], [], []
        for g in range(groups):
            dre, dim, fre, fim = (
                to_col(v[g : g + 1, :]) for v in (decay_re, decay_im, factor_re, factor_im)
            )
            m0, m1 = imap[layer, 0, g], imap[layer, 1, g]
            res.append(fre * m0 - fim * m1)
            ims.append(fre * m1 + fim * m0)
            s0, s1 = carried[layer, 0, g], carried[layer, 1, g]
            kept_re = jnp.where(live_row, dre * s0 - dim * s1, s0)
            kept_im = jnp.where(live_row, dre * s1 + dim * s0, s1)
            carried[layer, 0, g] = kept_re
            carried[layer, 1, g] = kept_im
            bases.append(
                dot_nn(omap[layer, 0, g], kept_re, HIGH) - dot_nn(omap[layer, 1, g], kept_im, HIGH)
            )
        cat_re = jnp.concatenate(res, axis=1) if groups > 1 else res[0]
        cat_im = jnp.concatenate(ims, axis=1) if groups > 1 else ims[0]
        owner = lax.broadcasted_iota(jnp.int32, cat_re.shape, 1)
        for g in range(groups):
            mine = (owner >= g * per) & (owner < (g + 1) * per)
            map_re = jnp.where(mine, cat_re, 0.0)
            map_im = jnp.where(mine, cat_im, 0.0)
            push_map[layer, 0, g] = map_re
            push_map[layer, 1, g] = map_im
            direct[layer, pl.ds(g * per, per), :] = dot_nn(
                omap[layer, 0, g], map_re, HIGH
            ) - dot_nn(omap[layer, 1, g], map_im, HIGH)
        base_t = jnp.concatenate(bases, axis=0) if groups > 1 else bases[0]
        base[layer] = dot_nt(jnp.where(eye(batch), 1.0, 0.0), base_t, HIGH)

    def advance(layer, drive):
        for g in range(groups):
            for part in range(2):
                push = dot_nt(push_map[layer, part, g], drive, HIGH)
                kept = carried[layer, part, g]
                carried[layer, part, g] = jnp.where(live_row, kept + push, kept)
        out = pltpu.make_async_copy(carried.at[layer], states_out.at[layer], out_sem.at[layer])
        out.start()
        return out

    def cols(ref, layer, slot, size):
        if isinstance(slot, int):
            return ref[layer, :, slot * size : (slot + 1) * size]
        return ref[layer, :, pl.ds(pl.multiple_of(slot * size, size), size)]

    def wide(buf, layer):
        return jnp.concatenate([buf[layer, k] for k in range(n)], axis=1)

    xbuf[0, me] = tokens[...]
    pl.semaphore_wait(barrier, len(greeted))

    outs = []
    k = start(0, xbuf.at[0])
    loads["imap"].wait()
    loads["omap"].wait()
    loads["states"].wait()
    prepare(0)
    for layer in range(layers):
        phase = 4 * layer
        loads["in", layer].wait()
        sums = [jnp.zeros((batch, width), jnp.float32), jnp.zeros((batch, chans), jnp.float32)]

        def take_x(slot):
            x = xbuf[layer, slot].astype(jnp.float32)
            if isinstance(slot, int):
                g = gain[layer : layer + 1, slot * width : (slot + 1) * width]
            else:
                g = gain[layer : layer + 1, pl.ds(pl.multiple_of(slot * width, width), width)]
            piece = (x * g).astype(jnp.bfloat16)
            scaled[slot] = piece
            sums[0] = sums[0] + x * x
            sums[1] = sums[1] + dot_nt(piece, cols(in_w, layer, slot, width))

        finish(phase, xbuf.at[layer], k, take_x if aligned else None)
        if not aligned:
            for slot in range(n):
                take_x(slot)
        inv = lax.rsqrt(jnp.sum(sums[0], axis=1, keepdims=True) / features + EPS)
        drive = inv * sums[1]
        response = dot_nt(drive, direct[layer], HIGH)
        read = base[layer] + jnp.where(live_col, response, 0.0) + skip[layer : layer + 1, :] * drive
        activated = jax.nn.gelu(read).astype(jnp.bfloat16)
        abuf[layer, me] = activated
        k = start(phase + 1, abuf.at[layer])

        loads["gate", layer].wait()
        gate_acc = jnp.zeros((batch, width), jnp.float32)
        for slot in range(n):
            gate_acc = gate_acc + dot_nt(scaled[slot], cols(gate_w, layer, slot, width))
        opening = jax.nn.sigmoid(inv * gate_acc)

        loads["glu", layer].wait()
        finish(phase + 1, abuf.at[layer], k)
        glu_pre = dot_nt(wide(abuf, layer), glu_w[layer])
        gated = (activated.astype(jnp.float32) * jax.nn.sigmoid(glu_pre)).astype(jnp.bfloat16)
        gbuf[layer, me] = gated
        k = start(phase + 2, gbuf.at[layer])

        outs.append(advance(layer, drive))

        loads["branch", layer].wait()
        finish(phase + 2, gbuf.at[layer], k)
        branch = dot_nt(wide(gbuf, layer), branch_w[layer])
        wbuf[layer, me] = (opening * branch).astype(jnp.bfloat16)
        k = start(phase + 3, wbuf.at[layer])

        if layer + 1 < layers:
            prepare(layer + 1)
        loads["mix", layer].wait()
        total = [jnp.zeros((batch, width), jnp.float32)]

        def take_w(slot):
            total[0] = total[0] + dot_nt(wbuf[layer, slot], cols(mix_w, layer, slot, width))

        finish(phase + 3, wbuf.at[layer], k, take_w if aligned else None)
        if not aligned:
            for slot in range(n):
                take_w(slot)
        x_own = xbuf[layer, me].astype(jnp.float32)
        result = jnp.where(live_col, x_own + total[0], x_own).astype(jnp.bfloat16)
        if layer + 1 < layers:
            xbuf[layer + 1, me] = result
            k = start(phase + 4, xbuf.at[layer + 1])
        else:
            mixed[...] = result
    for copy in sends:
        copy.wait_send()
    for copy in outs:
        copy.wait()


def split_of(n):
    cs = 2 if n % 2 == 0 else 1
    ys = 2 if (n // cs) % 2 == 0 else 1
    return n // (cs * ys), ys, cs


def per_device(
    n,
    tokens,
    lengths,
    norm_gain,
    in_weight,
    gate_weight,
    decay_rate,
    frequency,
    log_step,
    input_map,
    output_map,
    skip_scale,
    glu_weight,
    branch_weight,
    mix_weight,
    states,
):
    batch, width = tokens.shape
    layers = in_weight.shape[0]
    groups, per = input_map.shape[2], input_map.shape[4]
    size = input_map.shape[3]
    chans = groups * per
    vmem = pl.BlockSpec(memory_space=pltpu.VMEM)
    hbm = pl.BlockSpec(memory_space=pl.ANY)
    bf16, f32 = jnp.bfloat16, jnp.float32
    return pl.pallas_call(
        functools.partial(kernel, (layers, *split_of(n))),
        out_shape=(
            jax.ShapeDtypeStruct(tokens.shape, bf16),
            jax.ShapeDtypeStruct(states.shape, f32),
        ),
        in_specs=[vmem] * 7 + [hbm] * 8,
        out_specs=(vmem, hbm),
        scratch_shapes=[
            pltpu.VMEM(in_weight.shape, bf16),
            pltpu.VMEM(gate_weight.shape, bf16),
            pltpu.VMEM(glu_weight.shape, bf16),
            pltpu.VMEM(branch_weight.shape, bf16),
            pltpu.VMEM(mix_weight.shape, bf16),
            pltpu.VMEM(input_map.shape, f32),
            pltpu.VMEM(output_map.shape, f32),
            pltpu.VMEM(states.shape, f32),
            pltpu.VMEM((layers, n, batch, width), bf16),
            pltpu.VMEM((layers, n, batch, chans), bf16),
            pltpu.VMEM((layers, n, batch, chans), bf16),
            pltpu.VMEM((layers, n, batch, width), bf16),
            pltpu.VMEM((n, batch, width), bf16),
            pltpu.VMEM((layers, 2, groups, size, chans), f32),
            pltpu.VMEM((layers, chans, chans), f32),
            pltpu.VMEM((layers, batch, chans), f32),
            pltpu.SemaphoreType.DMA((3 + 5 * layers,)),
            pltpu.SemaphoreType.DMA((layers,)),
            pltpu.SemaphoreType.DMA((4 * layers, n)),
            pltpu.SemaphoreType.DMA((4 * layers, n)),
        ],
        compiler_params=pltpu.CompilerParams(collective_id=0, has_side_effects=True),
        name="decode_layers",
    )(
        tokens,
        lengths.reshape(1, batch),
        norm_gain,
        skip_scale,
        decay_rate,
        frequency,
        log_step,
        in_weight,
        gate_weight,
        input_map,
        output_map,
        glu_weight,
        branch_weight,
        mix_weight,
        states,
    )


def solution(mesh):
    in_specs = (
        P("grp", "tp"),
        P("grp"),
        P(),
        P(None, "tp", None),
        P(None, "tp", None),
        P(None, "tp", None),
        P(None, "tp", None),
        P(None, "tp"),
        P(None, None, "tp", None, None),
        P(None, None, "tp", None, None),
        P(None, "tp"),
        P(None, "tp", None),
        P(None, "tp", None),
        P(None, "tp", None),
        P(None, None, "tp", None, "grp"),
    )
    out_specs = (P("grp", "tp"), P(None, None, "tp", None, "grp"))
    return jax.shard_map(
        functools.partial(per_device, mesh.shape["tp"]),
        mesh=mesh,
        in_specs=in_specs,
        out_specs=out_specs,
        check_vma=False,
    )
```

time: 177 us -> 83.3 us (0.47)
  blocking collectives: 158 us -> 0 us
  Pallas kernels: 0 us -> 77.1 us
  matrix products: 10.5 us -> 0 us
  other arithmetic: 4.53 us -> 0 us
  local copies, waits for them, and re-layouts: 2.76 us -> 5.17 us
    all_gather x8 -> x0, blocking collectives: 158 us -> none  [the longest x2 45.1 us: one_layer(): lax.all_gather(current, 'tp', axis=1, tiled=True).astype(jnp.float32)]
    pallas_call x0 -> x1, Pallas kernels: none -> 77.1 us  [per_device(): pl.pallas_call(functools.partial(kernel, (layers, *split_of(n))), out_sha...]
    dot_general x18 -> x0, matrix products: 10.5 us -> none  [the longest x10 7.91 us: contract_piece(): lax.dot_general(piece, weight, (((1,), (1,)), ((), ())), preferred_elemen...]
    unnamed x20 -> x3, local copies, waits for them, and re-layouts: 0.04 us -> 5.17 us
    div x3 -> x0, other arithmetic: 2.37 us -> none  [the longest x2 1.66 us: discretize(): factor_re = ((decay_re - 1.0) * real_part + decay_im * frequency) / denom]
where the time goes in v1:
time: 83.3 us; the launch traced here: 82.9 us
  Pallas kernels  77.1 us (93%)
  local copies, waits for them, and re-layouts  5.17 us (6%)
    pallas_call x1, Pallas kernels, per_device(): pl.pallas_call(functools.partial(kernel, (layers, *split_of(n))), out_sha...  77.1 us
    unnamed x3, local copies, waits for them, and re-layouts  5.17 us

profile of v1, /device:TPU:0, one launch (start us, length us, event | category | flops | bytes accessed | tf_op | source)
XLA Modules:
  0.0 82.9 jit_solution(6871252434484427630)
XLA Ops:
  0.6 1.9 %copy.17.input_hbm = f32[2,2,4,64,16]{4,3,2,1,0:T(8,128)} copy(f32[2,2,4,64,16]{3,4,2,1,0:T(8,128)} %param.23) | data formatting | bytes 131072 | tf_op args[8]
  2.5 77.1 %decode_layers.1 = (bf16[64,256]{1,0:T(8,128)(2,1)}, f32[2,2,4,64,64]{4,3,2,1,0:T(8,128)}) custom-call(bf16[64,256]{1,0:T(8,128)(2,1)} %tokens.1, s32[1,64]{1,0:T(1,128)} %bitcast.1, f32[2,4096]{1,0:T(2,128)} %gain.1, f32[2,64]{1,0:T(2,128)} %skip.1, f32[2,4,64]{2,1,0:T(4,128)} %decay_rate.1, f32[2,4,64]{2,1,0:T(4,128)} %frequency.1, f32[2,4]{1,0:T(2,128)} %log_step.1, ...), custom_call_target="tpu_custom_call" | custom-call | tf_op jit(solution)/shard_map/decode_layers/pallas_call | solution.py:386
  79.7 1.4 %copy.20 = bf16[64,256]{1,0:T(8,128)(2,1)} copy(bf16[64,256]{1,0:T(8,128)(2,1)} %get-tuple-element.4) | data formatting | bytes 65536
  81.1 1.9 %copy.21 = f32[2,2,4,64,64]{4,3,2,1,0:T(8,128)} copy(f32[2,2,4,64,64]{4,3,2,1,0:T(8,128)} %get-tuple-element.5) | data formatting | bytes 524288

commit v2 on v1

--- a/solution.py
+++ b/solution.py
@@ -11,6 +11,7 @@
 EPS = 1e-06
 HIGH = lax.Precision.HIGHEST
 MESH = pl.DeviceIdType.MESH
+ROUTES = ("chip", "chip", "chip", "chip")
 
 
 def dot_nt(a, b, precision=None):
@@ -84,7 +85,7 @@
     batch, width = tokens.shape
     features = width * n
     groups = decay_rate.shape[1]
-    per = imap.shape[-1]
+    per = imap.shape[-2]
     chans = groups * per
     aligned = width % 128 == 0
 
@@ -96,12 +97,45 @@
     def place(z, y, c):
         return (z * ys + y) * cs + c
 
-    hops = sorted(range(1, zs), key=lambda d: (min(d, zs - d), d))
-    across = [lax.rem(zz + d, zs) for d in hops]
-    peers = [place(z, yy, core) for z in across]
-    other_y = place(zz, 1 - yy, core) if ys > 1 else None
-    partner = place(zz, yy, 1 - core) if cs > 1 else None
-    greeted = peers + [p for p in (other_y, partner) if p is not None]
+    hops = sorted(range(zs), key=lambda d: (min(d, zs - d), d))
+    partner = [place(zz, yy, 1 - core)] if cs > 1 else []
+
+    def away(dz, dy, dc):
+        return place(lax.rem(zz + dz, zs), yy if dy == 0 else 1 - yy, core if dc == 0 else 1 - core)
+
+    def route(kind):
+        chips = [(dz, dy) for dz in hops for dy in range(ys) if (dz, dy) != (0, 0)]
+        chips.sort(key=lambda h: min(h[0], zs - h[0]) + h[1])
+        far = [away(dz, dy, 1) for dz, dy in chips] if cs > 1 else []
+        if kind == "chip":
+            near = [away(dz, dy, 0) for dz, dy in chips]
+            return near[::-1] + partner, [(s, partner) for s in near] + [(s, []) for s in partner + far]
+        twin = zz + 1 - 2 * lax.rem(zz, 2)
+        across = [lax.rem(zz + d, zs) for d in range(2, zs, 2)]
+        beyond = [lax.rem(twin + d, zs) for d in range(2, zs, 2)]
+        side = away(0, 1, 0)
+
+        def both(c):
+            near = [place(twin, yy, c), place(twin, 1 - yy, c)]
+            return near, [place(z, yy, c) for z in across], [place(z, yy, c) for z in beyond]
+
+        near, column, outer = both(core)
+        slant = [place(z, 1 - yy, core) for z in beyond]
+        relayed = [place(z, 1 - yy, core) for z in across]
+        legs = [(s, partner) for s in [side] + near]
+        legs += [(s, [side] + partner) for s in column]
+        legs += [(s, partner) for s in outer + slant + relayed]
+        far = []
+        if cs > 1:
+            near2, column2, outer2 = both(1 - core)
+            far = [away(0, 1, 1)] + near2 + column2 + outer2
+            far += [place(z, 1 - yy, 1 - core) for z in beyond + across]
+        first = column + slant + outer + near[::-1] + [side] + partner
+        return first, legs + [(s, []) for s in partner + far]
+
+    pairable = ys > 1 and zs % 2 == 0
+    routes = [route(kind if kind != "mid" or pairable else "chip") for kind in ROUTES]
+    greeted = [away(dz, dy, 0) for dz in hops for dy in range(ys) if (dz, dy) != (0, 0)] + partner
 
     barrier = pltpu.get_barrier_semaphore()
     for p in greeted:
@@ -114,7 +148,6 @@
 
     loads = {}
     count = 0
-    plan = [("maps", None)]
     loads["imap"] = load(0, input_hbm, imap)
     loads["omap"] = load(1, output_hbm, omap)
     loads["states"] = load(2, states_hbm, carried)
@@ -150,11 +183,10 @@
         sends.append(copy)
 
     def start(phase, buf):
-        k = 0
-        for p in list(reversed(peers)) + [p for p in (other_y, partner) if p is not None]:
+        targets = routes[phase % 4][0]
+        for k, p in enumerate(targets):
             send(phase, buf, me, p, k)
-            k += 1
-        return k
+        return len(targets)
 
     def arrive(phase, buf, slot):
         pltpu.make_async_remote_copy(
@@ -167,46 +199,15 @@
         ).wait_recv()
 
     def finish(phase, buf, k, each=None):
-        def take(slot):
+        if each is not None:
+            each(me)
+        for slot, targets in routes[phase % 4][1]:
+            arrive(phase, buf, slot)
+            for p in targets:
+                send(phase, buf, slot, p, k)
+                k += 1
             if each is not None:
                 each(slot)
-
-        if each is not None:
-            each(me)
-        if ys > 1:
-            arrive(phase, buf, other_y)
-            if cs > 1:
-                send(phase, buf, other_y, partner, k)
-                k += 1
-            take(other_y)
-        for z in across:
-            slot = place(z, yy, core)
-            arrive(phase, buf, slot)
-            if ys > 1:
-                send(phase, buf, slot, other_y, k)
-                k += 1
-            if cs > 1:
-                send(phase, buf, slot, partner, k)
-                k += 1
-            take(slot)
-        if ys > 1:
-            for z in across:
-                slot = place(z, 1 - yy, core)
-                arrive(phase, buf, slot)
-                if cs > 1:
-                    send(phase, buf, slot, partner, k)
-                    k += 1
-                take(slot)
-        if cs > 1:
-            order = [place(zz, yy, 1 - core)]
-            if ys > 1:
-                order.append(place(zz, 1 - yy, 1 - core))
-            order += [place(z, yy, 1 - core) for z in across]
-            if ys > 1:
-                order += [place(z, 1 - yy, 1 - core) for z in across]
-            for slot in order:
-                arrive(phase, buf, slot)
-                take(slot)
 
     def prepare(layer):
         step = log_step[layer : layer + 1, :]
@@ -221,9 +222,8 @@
         factor_im = (decay_im * real - (decay_re - 1.0) * freq) / denom
         res, ims, bases = [], [], []
         for g in range(groups):
-            dre, dim, fre, fim = (
-                to_col(v[g : g + 1, :]) for v in (decay_re, decay_im, factor_re, factor_im)
-            )
+            dre, dim = to_col(decay_re[g : g + 1, :]), to_col(decay_im[g : g + 1, :])
+            fre, fim = factor_re[g : g + 1, :], factor_im[g : g + 1, :]
             m0, m1 = imap[layer, 0, g], imap[layer, 1, g]
             res.append(fre * m0 - fim * m1)
             ims.append(fre * m1 + fim * m0)
@@ -235,18 +235,19 @@
             bases.append(
                 dot_nn(omap[layer, 0, g], kept_re, HIGH) - dot_nn(omap[layer, 1, g], kept_im, HIGH)
             )
-        cat_re = jnp.concatenate(res, axis=1) if groups > 1 else res[0]
-        cat_im = jnp.concatenate(ims, axis=1) if groups > 1 else ims[0]
-        owner = lax.broadcasted_iota(jnp.int32, cat_re.shape, 1)
+        cat_re = jnp.concatenate(res, axis=0) if groups > 1 else res[0]
+        cat_im = jnp.concatenate(ims, axis=0) if groups > 1 else ims[0]
+        unit = jnp.where(eye(cat_re.shape[1]), 1.0, 0.0)
+        turned_re, turned_im = dot_nt(unit, cat_re, HIGH), dot_nt(unit, cat_im, HIGH)
+        owner = lax.broadcasted_iota(jnp.int32, turned_re.shape, 1)
+        source = lax.broadcasted_iota(jnp.int32, (per, chans), 1)
         for g in range(groups):
             mine = (owner >= g * per) & (owner < (g + 1) * per)
-            map_re = jnp.where(mine, cat_re, 0.0)
-            map_im = jnp.where(mine, cat_im, 0.0)
-            push_map[layer, 0, g] = map_re
-            push_map[layer, 1, g] = map_im
-            direct[layer, pl.ds(g * per, per), :] = dot_nn(
-                omap[layer, 0, g], map_re, HIGH
-            ) - dot_nn(omap[layer, 1, g], map_im, HIGH)
+            push_map[layer, 0, g] = jnp.where(mine, turned_re, 0.0)
+            push_map[layer, 1, g] = jnp.where(mine, turned_im, 0.0)
+            block = dot_nt(omap[layer, 0, g], cat_re, HIGH) - dot_nt(omap[layer, 1, g], cat_im, HIGH)
+            here = (source >= g * per) & (source < (g + 1) * per)
+            direct[layer, pl.ds(g * per, per), :] = jnp.where(here, block, 0.0)
         base_t = jnp.concatenate(bases, axis=0) if groups > 1 else bases[0]
         base[layer] = dot_nt(jnp.where(eye(batch), 1.0, 0.0), base_t, HIGH)
 
@@ -265,8 +266,16 @@
             return ref[layer, :, slot * size : (slot + 1) * size]
         return ref[layer, :, pl.ds(pl.multiple_of(slot * size, size), size)]
 
+    half = batch // 2
+
+    def pack(block):
+        return jnp.concatenate([block[:half], block[half:]], axis=1)
+
     def wide(buf, layer):
-        return jnp.concatenate([buf[layer, k] for k in range(n)], axis=1)
+        blocks = [buf[layer, k] for k in range(n)]
+        top = jnp.concatenate([block[:, :chans] for block in blocks], axis=1)
+        low = jnp.concatenate([block[:, chans:] for block in blocks], axis=1)
+        return jnp.concatenate([top, low], axis=0)
 
     xbuf[0, me] = tokens[...]
     pl.semaphore_wait(barrier, len(greeted))
@@ -302,7 +311,7 @@
         response = dot_nt(drive, direct[layer], HIGH)
         read = base[layer] + jnp.where(live_col, response, 0.0) + skip[layer : layer + 1, :] * drive
         activated = jax.nn.gelu(read).astype(jnp.bfloat16)
-        abuf[layer, me] = activated
+        abuf[layer, me] = pack(activated)
         k = start(phase + 1, abuf.at[layer])
 
         loads["gate", layer].wait()
@@ -315,7 +324,7 @@
         finish(phase + 1, abuf.at[layer], k)
         glu_pre = dot_nt(wide(abuf, layer), glu_w[layer])
         gated = (activated.astype(jnp.float32) * jax.nn.sigmoid(glu_pre)).astype(jnp.bfloat16)
-        gbuf[layer, me] = gated
+        gbuf[layer, me] = pack(gated)
         k = start(phase + 2, gbuf.at[layer])
 
         outs.append(advance(layer, drive))
@@ -349,6 +358,11 @@
         copy.wait_send()
     for copy in outs:
         copy.wait()
+
+
+def hand_over(mixed, states, mixed_out, states_out):
+    mixed_out[...] = mixed[...]
+    states_out[...] = states[...]
 
 
 def split_of(n):
@@ -383,7 +397,7 @@
     vmem = pl.BlockSpec(memory_space=pltpu.VMEM)
     hbm = pl.BlockSpec(memory_space=pl.ANY)
     bf16, f32 = jnp.bfloat16, jnp.float32
-    return pl.pallas_call(
+    mixed, finals = pl.pallas_call(
         functools.partial(kernel, (layers, *split_of(n))),
         out_shape=(
             jax.ShapeDtypeStruct(tokens.shape, bf16),
@@ -397,12 +411,12 @@
             pltpu.VMEM(glu_weight.shape, bf16),
             pltpu.VMEM(branch_weight.shape, bf16),
             pltpu.VMEM(mix_weight.shape, bf16),
-            pltpu.VMEM(input_map.shape, f32),
+            pltpu.VMEM((layers, 2, groups, per, size), f32),
             pltpu.VMEM(output_map.shape, f32),
             pltpu.VMEM(states.shape, f32),
             pltpu.VMEM((layers, n, batch, width), bf16),
-            pltpu.VMEM((layers, n, batch, chans), bf16),
-            pltpu.VMEM((layers, n, batch, chans), bf16),
+            pltpu.VMEM((layers, n, batch // 2, 2 * chans), bf16),
+            pltpu.VMEM((layers, n, batch // 2, 2 * chans), bf16),
             pltpu.VMEM((layers, n, batch, width), bf16),
             pltpu.VMEM((n, batch, width), bf16),
             pltpu.VMEM((layers, 2, groups, size, chans), f32),
@@ -425,13 +439,23 @@
         log_step,
         in_weight,
         gate_weight,
-        input_map,
+        jnp.swapaxes(input_map, 3, 4),
         output_map,
         glu_weight,
         branch_weight,
         mix_weight,
         states,
     )
+    return pl.pallas_call(
+        hand_over,
+        out_shape=(
+            jax.ShapeDtypeStruct(tokens.shape, bf16),
+            jax.ShapeDtypeStruct(states.shape, f32),
+        ),
+        in_specs=[vmem] * 2,
+        out_specs=(vmem,) * 2,
+        name="hand_over",
+    )(mixed, finals)
 
 
 def solution(mesh):

time: 83.3 us -> 66.4 us (0.80)
  Pallas kernels: 77.1 us -> 65.6 us
  local copies, waits for them, and re-layouts: 5.17 us -> 0 us
    pallas_call x1, Pallas kernels: 77.1 us -> 63.7 us  [per_device(): pl.pallas_call(functools.partial(kernel, (layers, *split_of(n))), out_sha...]
    unnamed x3 -> x0, local copies, waits for them, and re-layouts: 5.17 us -> none
    pallas_call x0 -> x1, Pallas kernels: none -> 1.89 us  [per_device(): pl.pallas_call(hand_over, out_shape=(jax.ShapeDtypeStruct(tokens.shape, b...]
where the time goes in v2:
time: 66.4 us; the launch traced here: 66.2 us
  Pallas kernels  65.6 us (99%)
    pallas_call x1, Pallas kernels, per_device(): pl.pallas_call(functools.partial(kernel, (layers, *split_of(n))), out_sha...  63.7 us
    pallas_call x1, Pallas kernels, per_device(): pl.pallas_call(hand_over, out_shape=(jax.ShapeDtypeStruct(tokens.shape, b...  1.89 us

profile of v2, /device:TPU:0, one launch (start us, length us, event | category | flops | bytes accessed | tf_op | source)
XLA Modules:
  0.0 66.2 jit_solution(6334079411912444623)
XLA Ops:
  0.6 63.7 %decode_layers.1 = (bf16[64,256]{1,0:T(8,128)(2,1)}, f32[2,2,4,64,64]{4,3,2,1,0:T(8,128)}) custom-call(bf16[64,256]{1,0:T(8,128)(2,1)} %tokens.1, s32[1,64]{1,0:T(1,128)} %bitcast.3, f32[2,4096]{1,0:T(2,128)} %gain.1, f32[2,64]{1,0:T(2,128)} %skip.1, f32[2,4,64]{2,1,0:T(4,128)} %decay_rate.1, f32[2,4,64]{2,1,0:T(4,128)} %frequency.1, f32[2,4]{1,0:T(2,128)} %log_step.1, ...), custom_call_target="tpu_custom_call" | custom-call | tf_op jit(solution)/shard_map/decode_layers/pallas_call | solution.py:400
  64.3 1.9 %hand_over.1 = (bf16[64,256]{1,0:T(8,128)(2,1)}, f32[2,2,4,64,64]{4,3,2,1,0:T(8,128)}) custom-call(bf16[64,256]{1,0:T(8,128)(2,1)} %get-tuple-element.4.mixed, f32[2,2,4,64,64]{4,3,2,1,0:T(8,128)} %get-tuple-element.5.states), custom_call_target="tpu_custom_call" | custom-call | tf_op jit(solution)/shard_map/hand_over/pallas_call | solution.py:449
